TPU v7x, 256 devices: a whole 4x4x8 slice. The times are simulated.
256 devices in a mesh: ra: 32 (over z, y), cb: 8 (over x, core).
Axes of the slice: x: 4, y: 4, z: 8, core: 2. Of those that a mesh axis runs over, the one named last changes fastest.
Arguments:
- tokens: bfloat16 [2048, 16384], P('ra'), may hold values from -16 to 16
- norm_gain: float32 [2, 2048], replicated, may hold values from 0.1 to 1.9
- up_weight: float32 [2, 2048, 6144], P(None, 'ra', 'cb'), may hold values from -0.125 to 0.125
- gate_weight: float32 [2, 2048, 6144], P(None, 'ra', 'cb'), may hold values from -0.125 to 0.125
- up_scale: float32 [2, 6144], P(None, 'cb'), may hold values from 0.5 to 2
- gate_scale: float32 [2, 6144], P(None, 'cb'), may hold values from 0.5 to 2
- up_taps: float32 [2, 3, 6144], P(None, None, 'cb'), may hold values from -3 to 3
- gate_taps: float32 [2, 3, 6144], P(None, None, 'cb'), may hold values from -3 to 3
- down_weight: float32 [2, 2048, 6144], P(None, 'ra', 'cb'), may hold values from -0.078125 to 0.078125
- down_scale: float32 [2, 2048], replicated, may hold values from 0.5 to 2
Outputs:
- mixed: bfloat16 [2048, 16384], P('ra')
All inputs are finite; a program needn't handle non-finite values.
Results may differ from a plain program's by a relative error of at most 0.024.
Values may be sent and summed in bfloat16 or wider, within the bound.
No kernel may reach another device: no remote copies, remote signals or barrier semaphores. Data moves between devices by JAX's collectives and lax.ppermute only.
A program may use at most 64 MiB of HBM per device.

v0:
```python
import jax
import jax.numpy as jnp
from jax import lax
from jax.sharding import Mesh
from jax.sharding import PartitionSpec as P

RA = ("z", "y")
CB = ("x", "c")
EPS = 1e-06
RESIDUAL = 0.5
BF = jnp.bfloat16
F32 = jnp.float32


def turned(value, axis, steps):
    count = lax.axis_size(axis)
    return lax.ppermute(value, axis, [(s, (s + steps) % count) for s in range(count)])


def shifted(value, axis, steps):
    count = lax.axis_size(axis)
    initial, last = (max(0, -steps), min(count, count - steps))
    return lax.ppermute(value, axis, [(s, s + steps) for s in range(initial, last)])


def at(blocks, index):
    return lax.dynamic_index_in_dim(blocks, index, 0, keepdims=False)


def gather_cb(own):
    half = own.shape[0] // 2
    x = lax.axis_index("x")
    c = lax.axis_index("c")
    left = turned(own, "x", 1)
    right = turned(own, "x", -1)
    far_low = turned(left[:half], "x", 1)
    far_high = turned(right[half:], "x", -1)
    far = jnp.concatenate([far_low, far_high], axis=0)
    whole = jnp.zeros((4, *own.shape), own.dtype)
    for steps, block in ((0, own), (3, left), (1, right), (2, far)):
        whole = lax.dynamic_update_index_in_dim(whole, block, (x + steps) % 4, 0)
    other = turned(whole, "c", 1)
    first = jnp.where(c == 0, whole, other)
    second = jnp.where(c == 0, other, whole)
    return jnp.stack([first, second], axis=1)


def scatter_cb(parts):
    x = lax.axis_index("x")
    c = lax.axis_index("c")
    mine = jnp.where(c == 0, parts[:, 0], parts[:, 1])
    sent = jnp.where(c == 0, parts[:, 1], parts[:, 0])
    pair = (mine.astype(F32) + turned(sent, "c", 1).astype(F32)).astype(BF)
    half = pair.shape[1] // 2
    far = at(pair, (x + 2) % 4)
    from_left = turned(far[:half], "x", 1)
    from_right = turned(far[half:], "x", -1)
    to_right = at(pair, (x + 1) % 4)
    to_left = at(pair, (x + 3) % 4)
    low = (to_right[:half].astype(F32) + from_left.astype(F32)).astype(BF)
    high = (to_left[half:].astype(F32) + from_right.astype(F32)).astype(BF)
    a = turned(jnp.concatenate([low, to_right[half:]], axis=0), "x", 1)
    b = turned(jnp.concatenate([to_left[:half], high], axis=0), "x", -1)
    return at(pair, x).astype(F32) + a.astype(F32) + b.astype(F32)


def valid_taps(values, taps):
    width = taps.shape[0]
    length = values.shape[0] - width + 1
    total = taps[0][None, :] * values[0:length]
    for k in range(1, width):
        total = total + taps[k][None, :] * values[k : k + length]
    return total


def per_device(
    tokens,
    norm_gain,
    up_weight,
    gate_weight,
    up_scale,
    gate_scale,
    up_taps,
    gate_taps,
    down_weight,
    down_scale,
):
    layers = up_weight.shape[0]
    ra = lax.axis_size("z") * lax.axis_size("y")
    cb = lax.axis_index("x") * 2 + lax.axis_index("c")
    rows, hid = up_weight.shape[1:]
    width = rows * ra
    part = rows // 8
    span = tokens.shape[1] // ra
    shards = [
        jnp.concatenate([w[l].astype(BF) for w in (up_weight, gate_weight, down_weight)], axis=1)
        for l in range(layers)
    ]
    weights = [lax.all_gather(s, RA, axis=0, tiled=True) for s in shards]
    own = lax.dynamic_slice_in_dim(tokens, cb * part, part, 0)
    own = own.reshape(part, ra, span).transpose(1, 0, 2)
    own = lax.all_to_all(own, RA, split_axis=0, concat_axis=0, tiled=True)
    every = gather_cb(own)
    state = every.reshape(8, ra, part, span).transpose(3, 1, 0, 2).reshape(span, width)
    edge = up_taps.shape[1] - 1
    for l in range(layers):
        before = shifted(state[span - edge :], RA, 1)
        rows_all = jnp.concatenate([before, state], axis=0)
        rows_f = rows_all.astype(F32)
        inverse = lax.rsqrt(jnp.mean(rows_f * rows_f, axis=1, keepdims=True) + EPS)
        scaled = (rows_f * norm_gain[l][None, :]).astype(BF)
        w = weights[l]
        up_raw = jnp.dot(scaled, w[:, :hid], preferred_element_type=F32)
        gate_raw = jnp.dot(scaled, w[:, hid : 2 * hid], preferred_element_type=F32)
        conv_up = valid_taps(up_raw * inverse * up_scale[l][None, :], up_taps[l])
        conv_gate = valid_taps(gate_raw * inverse * gate_scale[l][None, :], gate_taps[l])
        hidden = (jax.nn.silu(conv_gate) * conv_up).astype(BF)
        down_w = w[:, 2 * hid :]
        if l + 1 < layers:
            down = lax.dot_general(
                hidden, down_w, (((1,), (1,)), ((), ())), preferred_element_type=F32
            ).astype(BF)
            piece = scatter_cb(down.reshape(4, 2, span // 8, width))
            held = lax.dynamic_slice_in_dim(state, cb * (span // 8), span // 8, 0)
            piece = (piece * down_scale[l][None, :] + RESIDUAL * held.astype(F32)).astype(BF)
            state = gather_cb(piece).reshape(span, width)
        else:
            down = lax.dot_general(
                down_w, hidden, (((1,), (1,)), ((), ())), preferred_element_type=F32
            ).astype(BF)
            down = down.reshape(ra, 4, 2, part, span).transpose(1, 2, 0, 3, 4)
            piece = scatter_cb(down)
            held = lax.dynamic_index_in_dim(
                state.reshape(span, ra, 8, part), cb, 2, keepdims=False
            ).transpose(1, 2, 0)
            scale = lax.dynamic_index_in_dim(
                down_scale[l].reshape(ra, 8, part), cb, 1, keepdims=False
            )
            piece = (piece * scale[:, :, None] + RESIDUAL * held.astype(F32)).astype(BF)
    piece = lax.all_to_all(piece, RA, split_axis=0, concat_axis=0, tiled=True)
    piece = piece.transpose(1, 0, 2).reshape(part, ra * span)
    return gather_cb(piece).reshape(rows, ra * span)


def solution(mesh):
    torus = Mesh(mesh.devices.reshape(8, 4, 4, 2), ("z", "y", "x", "c"))
    placed = (
        P(RA, None),
        P(),
        P(None, RA, CB),
        P(None, RA, CB),
        P(None, CB),
        P(None, CB),
        P(None, None, CB),
        P(None, None, CB),
        P(None, RA, CB),
        P(),
    )
    return jax.shard_map(
        per_device, mesh=torus, in_specs=placed, out_specs=P(RA, None), check_vma=False
    )
```

profile of v0, /device:TPU:1, one launch (start us, length us, event | category | flops | bytes accessed | tf_op | source)
XLA Modules:
  0.0 315.6 jit_solution(3003010898439355616)
XLA Ops:
  6.5 1.2 convert.21
  7.7 1.0 convert.22
  8.7 1.0 convert.20
  11.5 23.3 %all_to_all.10 = bf16[32,8,512]{2,1,0:T(8,128)(2,1)S(1)} all-to-all(bf16[32,8,512]{2,1,0:T(8,128)(2,1)S(1)} %bitcast.156), channel_id=1, replica_groups=mesh['z'=8,'y'=4,'x'=4,'c'=2] {'z','y'}, dimensions={0} | all-to-all | bytes 524288 | tf_op jit(solution)/shard_map/all_to_all | solution.py:102
  34.8 1.2 collective-permute-start
  36.0 1.5 collective-permute-start.1
  37.5 4.0 %collective-permute-done = bf16[32,8,512]{2,1,0:T(8,128)(2,1)S(1)} collective-permute-done((bf16[32,8,512]{2,1,0:T(8,128)(2,1)S(1)}, bf16[32,8,512]{2,1,0:T(8,128)(2,1)S(1)}, u32[]{:S(2)}, u32[]{:S(2)}) %collective-permute-start) | collective-permute-done | bytes 262176 | tf_op jit(solution)/shard_map/ppermute | solution.py:17
  41.7 2.7 collective-permute-start.3
  44.5 2.2 collective-permute-done.2
  46.7 4.6 %collective-permute-start.4 = (bf16[4,32,8,512]{3,2,1,0:T(8,128)(2,1)S(1)}, bf16[4,32,8,512]{3,2,1,0:T(8,128)(2,1)S(1)}, u32[]{:S(2)}, u32[]{:S(2)}) collective-permute-start(bf16[4,32,8,512]{3,2,1,0:T(8,128)(2,1)S(1)} %fusion.75), channel_id=1, source_target_pairs={{0,1},{1,0},{2,3},{3,2},{4,5},{5,4},{6,7},{7,6},{8,9},{9,8},{10,11... | collective-permute-start | bytes 3145736 | tf_op jit(solution)/shard_map/ppermute | solution.py:17
  51.5 2.1 collective-permute-done.4
  54.4 1.7 copy.53
  56.3 2.7 collective-permute-start.5
  59.0 1.9 copy.54
  61.2 1.5 fusion.1
  62.8 54.4 %all-gather.5.cloned.1.call-done = bf16[2048,2304]{1,0:T(8,128)(2,1)} async-done(((bf16[64,2304]{1,0:T(8,128)(2,1)}), bf16[2048,2304]{1,0:T(8,128)(2,1)}) %all-gather.5.cloned.1.call-update) | async-done | bytes 9437200 | tf_op jit(solution)/shard_map/all_gather | solution.py:99
  117.2 5.2 %multiply_multiply_fusion.3 = f32[514,768]{1,0:T(8,128)S(1)} fusion(bf16[2048,2304]{1,0:T(8,128)(2,1)} %all-gather.5.cloned.1.call-done, f32[768]{0:T(1024)S(1)} %get-tuple-element.18, f32[514]{0:T(1024)S(1)} %add_rsqrt_fusion.1, f32[2048]{0:T(1024)S(1)} %bitcast.163, bf16[512,2048]{0,1:T(8,128)(2,1)S(1)} %bitcast.144, bf16[2,2048]{0,1:T(8,128)(2,1)S(1)} %copy.55), kind=kOutput, calls=%fused_computation.36 | convolution fusion | flops 1624009728 | bytes 6843400 | tf_op jit(solution)/shard_map/dot_general | solution.py:114
  122.4 3.2 %multiply_multiply_fusion.2 = f32[514,768]{1,0:T(8,128)S(1)} fusion(bf16[2048,2304]{1,0:T(8,128)(2,1)S(1)} %copy-done.14, f32[768]{0:T(1024)S(1)} %get-tuple-element.19, f32[514]{0:T(1024)S(1)} %add_rsqrt_fusion.1, f32[2048]{0:T(1024)S(1)} %bitcast.164, bf16[512,2048]{0,1:T(8,128)(2,1)S(1)} %bitcast.145, bf16[2,2048]{0,1:T(8,128)(2,1)S(1)} %copy.55), kind=kOutput, calls=%fused_computation.35 | convolution fusion | flops 1624009728 | bytes 7362560 | tf_op jit(solution)/shard_map/dot_general | solution.py:113
  125.7 2.7 fusion.20
  128.4 1.2 fusion.87
  129.6 2.0 copy.68
  131.6 1.8 copy.69
  133.4 1.5 select_bitcast_fusion
  134.9 1.9 copy.58
  136.8 3.3 %collective-permute-start.6 = (bf16[4,64,2048]{2,1,0:T(8,128)(2,1)S(1)}, bf16[4,64,2048]{2,1,0:T(8,128)(2,1)}, u32[]{:S(2)}, u32[]{:S(2)}) collective-permute-start(bf16[4,64,2048]{2,1,0:T(8,128)(2,1)S(1)} %copy.58), channel_id=1, source_target_pairs={{0,1},{1,0},{2,3},{3,2},{4,5},{5,4},{6,7},{7,6},{8,9},{9,8},{10,11... | collective-permute-start | bytes 3145736 | tf_op jit(solution)/shard_map/ppermute | solution.py:17
  140.1 2.4 collective-permute-done.6
  142.5 2.7 copy.59
  145.2 3.1 fusion.4
  148.7 1.2 collective-permute-start.7
  150.0 1.5 collective-permute-start.9
  151.5 12.3 %collective-permute-done.7 = bf16[32,2048]{0,1:T(8,128)(2,1)S(1)} collective-permute-done((bf16[32,2048]{0,1:T(8,128)(2,1)S(1)}, bf16[32,2048]{0,1:T(8,128)(2,1)S(1)}, u32[]{:S(2)}, u32[]{:S(2)}) %collective-permute-start.7) | collective-permute-done | bytes 131104 | tf_op jit(solution)/shard_map/ppermute | solution.py:17
  165.7 1.9 collective-permute-start.10
  167.7 11.2 %collective-permute-done.8 = bf16[64,2048]{0,1:T(8,128)(2,1)S(1)} collective-permute-done((bf16[64,2048]{0,1:T(8,128)(2,1)S(1)}, bf16[64,2048]{0,1:T(8,128)(2,1)S(1)}, u32[]{:S(2)}, u32[]{:S(2)}) %collective-permute-start.8) | collective-permute-done | bytes 262176 | tf_op jit(solution)/shard_map/ppermute | solution.py:17
  178.8 1.7 fusion.55
  180.5 2.8 collective-permute-start.12
  183.7 9.4 %collective-permute-done.12 = bf16[64,2048]{0,1:T(8,128)(2,1)S(1)} collective-permute-done((bf16[64,2048]{0,1:T(8,128)(2,1)S(1)}, bf16[64,2048]{0,1:T(8,128)(2,1)S(1)}, u32[]{:S(2)}, u32[]{:S(2)}) %collective-permute-start.12) | collective-permute-done | bytes 262176 | tf_op jit(solution)/shard_map/ppermute | solution.py:17
  194.1 3.5 %collective-permute-start.14 = (bf16[32,2048]{0,1:T(8,128)(2,1)}, bf16[32,2048]{0,1:T(8,128)(2,1)S(1)}, u32[]{:S(2)}, u32[]{:S(2)}) collective-permute-start(bf16[32,2048]{0,1:T(8,128)(2,1)} %slice.372), channel_id=1, source_target_pairs={{0,6},{2,0},{4,2},{6,4},{1,7},{3,1},{5,3},{7,5},{8,14},{10,8},{12,... | collective-permute-start | bytes 393224 | tf_op jit(solution)/shard_map/ppermute | solution.py:17
  198.4 1.3 copy.61
  199.9 6.9 %collective-permute-done.14 = bf16[32,2048]{0,1:T(8,128)(2,1)S(1)} collective-permute-done((bf16[32,2048]{0,1:T(8,128)(2,1)}, bf16[32,2048]{0,1:T(8,128)(2,1)S(1)}, u32[]{:S(2)}, u32[]{:S(2)}) %collective-permute-start.14) | collective-permute-done | bytes 131104 | tf_op jit(solution)/shard_map/ppermute | solution.py:17
  206.9 3.9 %collective-permute-done.13 = bf16[32,2048]{0,1:T(8,128)(2,1)S(1)} collective-permute-done((bf16[32,2048]{0,1:T(8,128)(2,1)}, bf16[32,2048]{0,1:T(8,128)(2,1)S(1)}, u32[]{:S(2)}, u32[]{:S(2)}) %collective-permute-start.13) | collective-permute-done | bytes 131104 | tf_op jit(solution)/shard_map/ppermute | solution.py:17
  211.3 3.4 %collective-permute-start.15 = (bf16[4,64,2048]{2,1,0:T(8,128)(2,1)S(1)}, bf16[4,64,2048]{2,1,0:T(8,128)(2,1)S(1)}, u32[]{:S(2)}, u32[]{:S(2)}) collective-permute-start(bf16[4,64,2048]{2,1,0:T(8,128)(2,1)S(1)} %constant_dynamic-update-slice_fusion.1), channel_id=1, source_target_pairs={{0,1},{1,0},{2,3},{3,2},{4,5},{5,4},{6,7},{7,6},{8,9},{9,8},{10,11... | collective-permute-start | bytes 3145736 | tf_op jit(solution)/shard_map/ppermute | solution.py:17
  214.8 2.3 collective-permute-done.15
  217.4 2.2 collective-permute-start.16
  220.9 4.0 %multiply_multiply_fusion.1 = f32[514,768]{1,0:T(8,128)S(1)} fusion(bf16[2048,2304]{1,0:T(8,128)(2,1)} %all-gather.3.cloned.1.call-done, f32[2048]{0:T(1024)S(1)} %bitcast.161, f32[768]{0:T(1024)S(1)} %get-tuple-element.17, f32[514]{0:T(1024)S(1)} %add_rsqrt_fusion, bf16[512,2048]{1,0:T(8,128)(2,1)S(1)} %bitcast.139, ...), kind=kOutput, calls=%fused_computation.34 | convolution fusion | flops 1624009728 | bytes 6843400 | tf_op jit(solution)/shard_map/dot_general | solution.py:114
  225.5 2.0 multiply_multiply_fusion
  227.5 2.3 fusion.17
  230.0 1.3 copy-done.2
  231.5 1.3 collective-permute-start.17
  232.8 2.4 collective-permute-done.17
  235.2 2.3 fusion.23
  238.2 2.1 collective-permute-start.20
  240.3 3.2 %collective-permute-done.18 = bf16[16,8,512]{2,1,0:T(8,128)(2,1)S(1)} collective-permute-done((bf16[16,8,512]{2,1,0:T(8,128)(2,1)S(1)}, bf16[16,8,512]{2,1,0:T(8,128)(2,1)S(1)}, u32[]{:S(2)}, u32[]{:S(2)}) %collective-permute-start.18) | collective-permute-done | bytes 131104 | tf_op jit(solution)/shard_map/ppermute | solution.py:17
  244.7 2.6 collective-permute-start.21
  247.4 7.5 %copy.66 = bf16[4,2,64,2048]{2,1,0,3:T(2,128)(2,1)} copy(bf16[4,2,64,2048]{3,2,1,0:T(8,128)(2,1)S(1)} %pad_maximum_fusion.3) | data formatting | bytes 4194304 | tf_op jit(solution)/shard_map/stack | solution.py:45
  254.9 9.3 %reshape_reshape.3 = bf16[512,32,8,8]{0,3,2,1:T(8,128)(2,1)S(1)} reshape(bf16[4,2,64,2048]{2,1,0,3:T(2,128)(2,1)} %copy.66) | data formatting | bytes 4194304 | tf_op jit(solution)/shard_map/reshape;reshape | solution.py:134
  264.3 1.2 fusion.72
  265.5 19.9 %all_to_all.11 = bf16[32,8,512]{2,1,0:T(8,128)(2,1)S(1)} all-to-all(bf16[32,8,512]{2,1,0:T(8,128)(2,1)S(1)} %fusion.72), channel_id=1, replica_groups=mesh['z'=8,'y'=4,'x'=4,'c'=2] {'z','y'}, dimensions={0} | all-to-all | bytes 524288 | tf_op jit(solution)/shard_map/all_to_all | solution.py:140
  285.4 2.7 collective-permute-start.23
  288.2 3.6 %collective-permute-done.22 = bf16[8,16384]{1,0:T(8,128)(2,1)S(1)} collective-permute-done((bf16[8,16384]{1,0:T(8,128)(2,1)S(1)}, bf16[8,16384]{1,0:T(8,128)(2,1)S(1)}, u32[]{:S(2)}, u32[]{:S(2)}) %collective-permute-start.22) | collective-permute-done | bytes 262176 | tf_op jit(solution)/shard_map/ppermute | solution.py:17
  292.1 2.7 collective-permute-start.25
  294.9 2.6 collective-permute-done.24
  297.6 6.1 %collective-permute-start.26 = (bf16[4,8,16384]{2,1,0:T(8,128)(2,1)S(1)}, bf16[4,8,16384]{2,1,0:T(8,128)(2,1)S(1)}, u32[]{:S(2)}, u32[]{:S(2)}) collective-permute-start(bf16[4,8,16384]{2,1,0:T(8,128)(2,1)S(1)} %fusion.76), channel_id=1, source_target_pairs={{0,1},{1,0},{2,3},{3,2},{4,5},{5,4},{6,7},{7,6},{8,9},{9,8},{10,11... | collective-permute-start | bytes 3145736 | tf_op jit(solution)/shard_map/ppermute | solution.py:17
  303.8 2.3 collective-permute-done.26
  306.2 1.5 pad_maximum_fusion.4
  (113 shorter events, 14.5 us)
Async XLA Ops:
  6.5 4.9 %copy-start = (bf16[64,16384]{1,0:T(8,128)(2,1)S(1)}, bf16[64,16384]{1,0:T(8,128)(2,1)}, u32[]{:S(2)}) copy-start(bf16[64,16384]{1,0:T(8,128)(2,1)} %param.10) | copy-start | bytes 6291460
  6.5 110.7 %all-gather.5.cloned.1.call-start = ((), (), s32[]{:S(2)}) async-start(), calls=%async_computation.3 | async-start | bytes 9732096 | tf_op jit(solution)/shard_map/all_gather | solution.py:99
  10.6 210.3 %all-gather.3.cloned.1.call-start = ((), (), s32[]{:S(2)}) async-start(), calls=%async_computation.2 | async-start | bytes 9732096 | tf_op jit(solution)/shard_map/all_gather | solution.py:99
  11.4 39.9 %copy-start.11 = (f32[2,768]{1,0:T(2,128)S(1)}, f32[2,768]{1,0:T(2,128)}, u32[]{:S(2)}) copy-start(f32[2,768]{1,0:T(2,128)} %param.15) | copy-start | bytes 18436
  11.5 39.9 %copy-start.7 = (f32[2,3,768]{2,0,1:T(2,128)S(1)}, f32[2,3,768]{2,0,1:T(2,128)}, u32[]{:S(2)}) copy-start(f32[2,3,768]{2,0,1:T(2,128)} %param.16) | copy-start | bytes 55300
  11.5 39.9 %copy-start.8 = (f32[2,3,768]{2,0,1:T(2,128)S(1)}, f32[2,3,768]{2,0,1:T(2,128)}, u32[]{:S(2)}) copy-start(f32[2,3,768]{2,0,1:T(2,128)} %param.17) | copy-start | bytes 55300
  11.5 40.0 %copy-start.9 = (f32[2,2048]{1,0:T(2,128)S(1)}, f32[2,2048]{1,0:T(2,128)}, u32[]{:S(2)}) copy-start(f32[2,2048]{1,0:T(2,128)} %param.11) | copy-start | bytes 49156
  34.8 6.8 %collective-permute-start = (bf16[32,8,512]{2,1,0:T(8,128)(2,1)S(1)}, bf16[32,8,512]{2,1,0:T(8,128)(2,1)S(1)}, u32[]{:S(2)}, u32[]{:S(2)}) collective-permute-start(bf16[32,8,512]{2,1,0:T(8,128)(2,1)S(1)} %all_to_all.10), channel_id=1, source_target_pairs={{0,2},{2,4},{4,6},{6,0},{1,3},{3,5},{5,7},{7,1},{8,10},{10,12},{12... | collective-permute-start | bytes 786440 | tf_op jit(solution)/shard_map/ppermute | solution.py:17
  36.0 5.7 %collective-permute-start.1 = (bf16[32,8,512]{2,1,0:T(8,128)(2,1)S(1)}, bf16[32,8,512]{2,1,0:T(8,128)(2,1)S(1)}, u32[]{:S(2)}, u32[]{:S(2)}) collective-permute-start(bf16[32,8,512]{2,1,0:T(8,128)(2,1)S(1)} %all_to_all.10), channel_id=1, source_target_pairs={{0,6},{2,0},{4,2},{6,4},{1,7},{3,1},{5,3},{7,5},{8,14},{10,8},{12,... | collective-permute-start | bytes 786440 | tf_op jit(solution)/shard_map/ppermute | solution.py:17
  41.6 5.1 %collective-permute-start.2 = (bf16[16,8,512]{2,1,0:T(8,128)(2,1)S(1)}, bf16[16,8,512]{2,1,0:T(8,128)(2,1)S(1)}, u32[]{:S(2)}, u32[]{:S(2)}) collective-permute-start(bf16[16,8,512]{2,1,0:T(8,128)(2,1)S(1)} %slice.354), channel_id=1, source_target_pairs={{0,2},{2,4},{4,6},{6,0},{1,3},{3,5},{5,7},{7,1},{8,10},{10,12},{12... | collective-permute-start | bytes 393224 | tf_op jit(solution)/shard_map/ppermute | solution.py:17
  41.7 5.0 %collective-permute-start.3 = (bf16[16,8,512]{2,1,0:T(8,128)(2,1)S(1)}, bf16[16,8,512]{2,1,0:T(8,128)(2,1)S(1)}, u32[]{:S(2)}, u32[]{:S(2)}) collective-permute-start(bf16[16,8,512]{2,1,0:T(8,128)(2,1)S(1)} %slice.355), channel_id=1, source_target_pairs={{0,6},{2,0},{4,2},{6,4},{1,7},{3,1},{5,3},{7,5},{8,14},{10,8},{12,... | collective-permute-start | bytes 393224 | tf_op jit(solution)/shard_map/ppermute | solution.py:17
  46.7 6.9 %collective-permute-start.4 = (bf16[4,32,8,512]{3,2,1,0:T(8,128)(2,1)S(1)}, bf16[4,32,8,512]{3,2,1,0:T(8,128)(2,1)S(1)}, u32[]{:S(2)}, u32[]{:S(2)}) collective-permute-start(bf16[4,32,8,512]{3,2,1,0:T(8,128)(2,1)S(1)} %fusion.75), channel_id=1, source_target_pairs={{0,1},{1,0},{2,3},{3,2},{4,5},{5,4},{6,7},{7,6},{8,9},{9,8},{10,11... | collective-permute-start | bytes 3145736 | tf_op jit(solution)/shard_map/ppermute | solution.py:17
  53.9 5.0 %copy-start.12 = (f32[2,768]{1,0:T(2,128)S(1)}, f32[2,768]{1,0:T(2,128)}, u32[]{:S(2)}) copy-start(f32[2,768]{1,0:T(2,128)} %param.14) | copy-start | bytes 18436
  54.2 4.8 %copy-start.5 = (bf16[4,2,32,8,512]{4,3,2,1,0:T(8,128)(2,1)}, bf16[4,2,32,8,512]{4,3,2,1,0:T(8,128)(2,1)S(1)}, u32[]{:S(2)}) copy-start(bf16[4,2,32,8,512]{4,3,2,1,0:T(8,128)(2,1)S(1)} %copy.52) | copy-start | bytes 6291460
  56.3 4.6 %collective-permute-start.5 = (bf16[2,2048]{1,0:T(2,128)(2,1)S(1)}, bf16[2,2048]{1,0:T(2,128)(2,1)S(1)}, u32[]{:S(2)}, u32[]{:S(2)}) collective-permute-start(bf16[2,2048]{1,0:T(2,128)(2,1)S(1)} %slice.282), channel_id=1, source_target_pairs={{0,8},{8,16},{16,24},{24,32},{32,40},{40,48},{48,56},{56,64},{64,7... | collective-permute-start | bytes 24584 | tf_op jit(solution)/shard_map/ppermute | solution.py:23
  60.9 61.6 %copy-start.4 = (bf16[512,32,8,8]{0,3,2,1:T(8,128)(2,1)}, bf16[512,32,8,8]{0,3,2,1:T(8,128)(2,1)S(1)}, u32[]{:S(2)}) copy-start(bf16[512,32,8,8]{0,3,2,1:T(8,128)(2,1)S(1)} %copy.54) | copy-start | bytes 6291460
  117.2 5.2 %copy-start.14 = (bf16[2048,2304]{1,0:T(8,128)(2,1)S(1)}, bf16[2048,2304]{1,0:T(8,128)(2,1)}, u32[]{:S(2)}) copy-start(bf16[2048,2304]{1,0:T(8,128)(2,1)} %all-gather.5.cloned.1.call-done) | copy-start | bytes 28311556
  136.8 5.7 %collective-permute-start.6 = (bf16[4,64,2048]{2,1,0:T(8,128)(2,1)S(1)}, bf16[4,64,2048]{2,1,0:T(8,128)(2,1)}, u32[]{:S(2)}, u32[]{:S(2)}) collective-permute-start(bf16[4,64,2048]{2,1,0:T(8,128)(2,1)S(1)} %copy.58), channel_id=1, source_target_pairs={{0,1},{1,0},{2,3},{3,2},{4,5},{5,4},{6,7},{7,6},{8,9},{9,8},{10,11... | collective-permute-start | bytes 3145736 | tf_op jit(solution)/shard_map/ppermute | solution.py:17
  148.3 15.5 %copy-start.3 = (bf16[4,64,2048]{1,2,0:T(8,128)(2,1)}, bf16[4,64,2048]{1,2,0:T(8,128)(2,1)S(1)}, u32[]{:S(2)}) copy-start(bf16[4,64,2048]{1,2,0:T(8,128)(2,1)S(1)} %fusion.4) | copy-start | bytes 3145732
  148.7 15.1 %collective-permute-start.7 = (bf16[32,2048]{0,1:T(8,128)(2,1)S(1)}, bf16[32,2048]{0,1:T(8,128)(2,1)S(1)}, u32[]{:S(2)}, u32[]{:S(2)}) collective-permute-start(bf16[32,2048]{0,1:T(8,128)(2,1)S(1)} %get-tuple-element.27), channel_id=1, source_target_pairs={{0,2},{2,4},{4,6},{6,0},{1,3},{3,5},{5,7},{7,1},{8,10},{10,12},{12... | collective-permute-start | bytes 393224 | tf_op jit(solution)/shard_map/ppermute | solution.py:17
  150.0 13.8 %collective-permute-start.9 = (bf16[32,2048]{0,1:T(8,128)(2,1)S(1)}, bf16[32,2048]{0,1:T(8,128)(2,1)S(1)}, u32[]{:S(2)}, u32[]{:S(2)}) collective-permute-start(bf16[32,2048]{0,1:T(8,128)(2,1)S(1)} %get-tuple-element.29), channel_id=1, source_target_pairs={{0,6},{2,0},{4,2},{6,4},{1,7},{3,1},{5,3},{7,5},{8,14},{10,8},{12,... | collective-permute-start | bytes 393224 | tf_op jit(solution)/shard_map/ppermute | solution.py:17
  164.2 3.4 %copy-start.10 = (f32[2,2048]{1,0:T(2,128)S(1)}, f32[2,2048]{1,0:T(2,128)}, u32[]{:S(2)}) copy-start(f32[2,2048]{1,0:T(2,128)} %param.19) | copy-start | bytes 49156
  164.5 14.3 %collective-permute-start.8 = (bf16[64,2048]{0,1:T(8,128)(2,1)S(1)}, bf16[64,2048]{0,1:T(8,128)(2,1)S(1)}, u32[]{:S(2)}, u32[]{:S(2)}) collective-permute-start(bf16[64,2048]{0,1:T(8,128)(2,1)S(1)} %pad_maximum_fusion.7), channel_id=1, source_target_pairs={{0,2},{2,4},{4,6},{6,0},{1,3},{3,5},{5,7},{7,1},{8,10},{10,12},{12... | collective-permute-start | bytes 786440 | tf_op jit(solution)/shard_map/ppermute | solution.py:17
  165.7 13.1 %collective-permute-start.10 = (bf16[64,2048]{0,1:T(8,128)(2,1)S(1)}, bf16[64,2048]{0,1:T(8,128)(2,1)S(1)}, u32[]{:S(2)}, u32[]{:S(2)}) collective-permute-start(bf16[64,2048]{0,1:T(8,128)(2,1)S(1)} %pad_maximum_fusion.8), channel_id=1, source_target_pairs={{0,6},{2,0},{4,2},{6,4},{1,7},{3,1},{5,3},{7,5},{8,14},{10,8},{12,... | collective-permute-start | bytes 786440 | tf_op jit(solution)/shard_map/ppermute | solution.py:17
  180.5 12.5 %collective-permute-start.12 = (bf16[64,2048]{0,1:T(8,128)(2,1)S(1)}, bf16[64,2048]{0,1:T(8,128)(2,1)S(1)}, u32[]{:S(2)}, u32[]{:S(2)}) collective-permute-start(bf16[64,2048]{0,1:T(8,128)(2,1)S(1)} %fusion.55), channel_id=1, source_target_pairs={{0,6},{2,0},{4,2},{6,4},{1,7},{3,1},{5,3},{7,5},{8,14},{10,8},{12,... | collective-permute-start | bytes 786440 | tf_op jit(solution)/shard_map/ppermute | solution.py:17
  183.4 14.2 %collective-permute-start.11 = (bf16[64,2048]{0,1:T(8,128)(2,1)S(1)}, bf16[64,2048]{0,1:T(8,128)(2,1)S(1)}, u32[]{:S(2)}, u32[]{:S(2)}) collective-permute-start(bf16[64,2048]{0,1:T(8,128)(2,1)S(1)} %fusion.55), channel_id=1, source_target_pairs={{0,2},{2,4},{4,6},{6,0},{1,3},{3,5},{5,7},{7,1},{8,10},{10,12},{12... | collective-permute-start | bytes 786440 | tf_op jit(solution)/shard_map/ppermute | solution.py:17
  194.1 12.8 %collective-permute-start.14 = (bf16[32,2048]{0,1:T(8,128)(2,1)}, bf16[32,2048]{0,1:T(8,128)(2,1)S(1)}, u32[]{:S(2)}, u32[]{:S(2)}) collective-permute-start(bf16[32,2048]{0,1:T(8,128)(2,1)} %slice.372), channel_id=1, source_target_pairs={{0,6},{2,0},{4,2},{6,4},{1,7},{3,1},{5,3},{7,5},{8,14},{10,8},{12,... | collective-permute-start | bytes 393224 | tf_op jit(solution)/shard_map/ppermute | solution.py:17
  197.6 0.8 copy-start.6
  198.4 12.4 %collective-permute-start.13 = (bf16[32,2048]{0,1:T(8,128)(2,1)}, bf16[32,2048]{0,1:T(8,128)(2,1)S(1)}, u32[]{:S(2)}, u32[]{:S(2)}) collective-permute-start(bf16[32,2048]{0,1:T(8,128)(2,1)} %bitcast.157), channel_id=1, source_target_pairs={{0,2},{2,4},{4,6},{6,0},{1,3},{3,5},{5,7},{7,1},{8,10},{10,12},{12... | collective-permute-start | bytes 393224 | tf_op jit(solution)/shard_map/ppermute | solution.py:17
  211.3 5.7 %collective-permute-start.15 = (bf16[4,64,2048]{2,1,0:T(8,128)(2,1)S(1)}, bf16[4,64,2048]{2,1,0:T(8,128)(2,1)S(1)}, u32[]{:S(2)}, u32[]{:S(2)}) collective-permute-start(bf16[4,64,2048]{2,1,0:T(8,128)(2,1)S(1)} %constant_dynamic-update-slice_fusion.1), channel_id=1, source_target_pairs={{0,1},{1,0},{2,3},{3,2},{4,5},{5,4},{6,7},{7,6},{8,9},{9,8},{10,11... | collective-permute-start | bytes 3145736 | tf_op jit(solution)/shard_map/ppermute | solution.py:17
  217.4 2.6 collective-permute-start.16
  220.9 4.6 %copy-start.13 = (bf16[2048,2304]{1,0:T(8,128)(2,1)S(1)}, bf16[2048,2304]{1,0:T(8,128)(2,1)}, u32[]{:S(2)}) copy-start(bf16[2048,2304]{1,0:T(8,128)(2,1)} %all-gather.3.cloned.1.call-done) | copy-start | bytes 28311556
  230.0 1.3 copy-start.2
  231.5 3.7 %collective-permute-start.17 = (bf16[4,32,8,512]{3,2,1,0:T(8,128)(2,1)S(1)}, bf16[4,32,8,512]{3,2,1,0:T(8,128)(2,1)}, u32[]{:S(2)}, u32[]{:S(2)}) collective-permute-start(bf16[4,32,8,512]{3,2,1,0:T(8,128)(2,1)S(1)} %select_bitcast_fusion.3), channel_id=1, source_target_pairs={{0,1},{1,0},{2,3},{3,2},{4,5},{5,4},{6,7},{7,6},{8,9},{9,8},{10,11... | collective-permute-start | bytes 3145736 | tf_op jit(solution)/shard_map/ppermute | solution.py:17
  237.6 6.0 %collective-permute-start.18 = (bf16[16,8,512]{2,1,0:T(8,128)(2,1)S(1)}, bf16[16,8,512]{2,1,0:T(8,128)(2,1)S(1)}, u32[]{:S(2)}, u32[]{:S(2)}) collective-permute-start(bf16[16,8,512]{2,1,0:T(8,128)(2,1)S(1)} %get-tuple-element.37), channel_id=1, source_target_pairs={{0,2},{2,4},{4,6},{6,0},{1,3},{3,5},{5,7},{7,1},{8,10},{10,12},{12... | collective-permute-start | bytes 393224 | tf_op jit(solution)/shard_map/ppermute | solution.py:17
  238.2 5.4 %collective-permute-start.20 = (bf16[16,8,512]{2,1,0:T(8,128)(2,1)S(1)}, bf16[16,8,512]{2,1,0:T(8,128)(2,1)S(1)}, u32[]{:S(2)}, u32[]{:S(2)}) collective-permute-start(bf16[16,8,512]{2,1,0:T(8,128)(2,1)S(1)} %get-tuple-element.39), channel_id=1, source_target_pairs={{0,6},{2,0},{4,2},{6,4},{1,7},{3,1},{5,3},{7,5},{8,14},{10,8},{12,... | collective-permute-start | bytes 393224 | tf_op jit(solution)/shard_map/ppermute | solution.py:17
  243.6 20.6 %collective-permute-start.19 = (bf16[32,8,512]{2,1,0:T(8,128)(2,1)S(1)}, bf16[32,8,512]{2,1,0:T(8,128)(2,1)}, u32[]{:S(2)}, u32[]{:S(2)}) collective-permute-start(bf16[32,8,512]{2,1,0:T(8,128)(2,1)S(1)} %pad_maximum_fusion.11), channel_id=1, source_target_pairs={{0,2},{2,4},{4,6},{6,0},{1,3},{3,5},{5,7},{7,1},{8,10},{10,12},{12... | collective-permute-start | bytes 786440 | tf_op jit(solution)/shard_map/ppermute | solution.py:17
  244.7 19.6 %collective-permute-start.21 = (bf16[32,8,512]{2,1,0:T(8,128)(2,1)}, bf16[32,8,512]{2,1,0:T(8,128)(2,1)}, u32[]{:S(2)}, u32[]{:S(2)}) collective-permute-start(bf16[32,8,512]{2,1,0:T(8,128)(2,1)} %pad_maximum_fusion.12), channel_id=1, source_target_pairs={{0,6},{2,0},{4,2},{6,4},{1,7},{3,1},{5,3},{7,5},{8,14},{10,8},{12,... | collective-permute-start | bytes 786440 | tf_op jit(solution)/shard_map/ppermute | solution.py:17
  285.4 6.4 %collective-permute-start.22 = (bf16[8,16384]{1,0:T(8,128)(2,1)S(1)}, bf16[8,16384]{1,0:T(8,128)(2,1)S(1)}, u32[]{:S(2)}, u32[]{:S(2)}) collective-permute-start(bf16[8,16384]{1,0:T(8,128)(2,1)S(1)} %bitcast.153), channel_id=1, source_target_pairs={{0,2},{2,4},{4,6},{6,0},{1,3},{3,5},{5,7},{7,1},{8,10},{10,12},{12... | collective-permute-start | bytes 786440 | tf_op jit(solution)/shard_map/ppermute | solution.py:17
  285.4 6.6 %collective-permute-start.23 = (bf16[8,16384]{1,0:T(8,128)(2,1)S(1)}, bf16[8,16384]{1,0:T(8,128)(2,1)S(1)}, u32[]{:S(2)}, u32[]{:S(2)}) collective-permute-start(bf16[8,16384]{1,0:T(8,128)(2,1)S(1)} %bitcast.154), channel_id=1, source_target_pairs={{0,6},{2,0},{4,2},{6,4},{1,7},{3,1},{5,3},{7,5},{8,14},{10,8},{12,... | collective-permute-start | bytes 786440 | tf_op jit(solution)/shard_map/ppermute | solution.py:17
  291.9 5.6 %collective-permute-start.24 = (bf16[4,16384]{1,0:T(4,128)(2,1)S(1)}, bf16[4,16384]{1,0:T(4,128)(2,1)S(1)}, u32[]{:S(2)}, u32[]{:S(2)}) collective-permute-start(bf16[4,16384]{1,0:T(4,128)(2,1)S(1)} %slice.384), channel_id=1, source_target_pairs={{0,2},{2,4},{4,6},{6,0},{1,3},{3,5},{5,7},{7,1},{8,10},{10,12},{12... | collective-permute-start | bytes 393224 | tf_op jit(solution)/shard_map/ppermute | solution.py:17
  292.1 5.4 %collective-permute-start.25 = (bf16[4,16384]{1,0:T(4,128)(2,1)S(1)}, bf16[4,16384]{1,0:T(4,128)(2,1)S(1)}, u32[]{:S(2)}, u32[]{:S(2)}) collective-permute-start(bf16[4,16384]{1,0:T(4,128)(2,1)S(1)} %slice.385), channel_id=1, source_target_pairs={{0,6},{2,0},{4,2},{6,4},{1,7},{3,1},{5,3},{7,5},{8,14},{10,8},{12,... | collective-permute-start | bytes 393224 | tf_op jit(solution)/shard_map/ppermute | solution.py:17
  297.6 8.4 %collective-permute-start.26 = (bf16[4,8,16384]{2,1,0:T(8,128)(2,1)S(1)}, bf16[4,8,16384]{2,1,0:T(8,128)(2,1)S(1)}, u32[]{:S(2)}, u32[]{:S(2)}) collective-permute-start(bf16[4,8,16384]{2,1,0:T(8,128)(2,1)S(1)} %fusion.76), channel_id=1, source_target_pairs={{0,1},{1,0},{2,3},{3,2},{4,5},{5,4},{6,7},{7,6},{8,9},{9,8},{10,11... | collective-permute-start | bytes 3145736 | tf_op jit(solution)/shard_map/ppermute | solution.py:17
  306.2 2.4 copy-start.1
Sparse Core Ops, SparseCore 0:
  10.7 106.4 all-gather.4
  119.8 100.2 all-gather.2
where the time goes:
time: 321 us; the launch traced here: 316 us
  waiting for transfers between devices  126 us (39%)
  starting transfers between devices  52.2 us (16%)
  blocking collectives  43.2 us (13%)
  local copies, waits for them, and re-layouts  39.1 us (12%)
  other arithmetic  21.6 us (7%)
  matrix products  19.4 us (6%)
  between operations  14.3 us (4%)
    ppermute x25, waiting for transfers between devices, turned(): lax.ppermute(value, axis, [(s, (s + steps) % count) for s in range(count)])  71 us
    all_gather x2, waiting for transfers between devices, per_device(): weights = [lax.all_gather(s, RA, axis=0, tiled=True) for s in shards]  54.4 us
    ppermute x25, starting transfers between devices, turned(): lax.ppermute(value, axis, [(s, (s + steps) % count) for s in range(count)])  47.3 us
    all_to_all x1, blocking collectives, per_device(): own = lax.all_to_all(own, RA, split_axis=0, concat_axis=0, tiled=True)  23.3 us
    all_to_all x1, blocking collectives, per_device(): piece = lax.all_to_all(piece, RA, split_axis=0, concat_axis=0, tiled=True)  19.9 us
    another operation x1, local copies, waits for them, and re-layouts, per_device(): state.reshape(span, ra, 8, part)  9.35 us
    dot_general x2, matrix products, per_device(): gate_raw = jnp.dot(scaled, w[:, hid:2 * hid], preferred_element_type=F32)  9.18 us
    another operation x2, local copies, waits for them, and re-layouts, gather_cb(): return jnp.stack([first, second], axis=1)  7.73 us
  transfers between devices with their start and end apart: 29, of which 17 were waited for; matrix products, arithmetic and copies ran while one was open for 19% of the time, Pallas kernels for 0%

commit v1 on v0

--- a/solution.py
+++ b/solution.py
@@ -10,6 +10,13 @@
 RESIDUAL = 0.5
 BF = jnp.bfloat16
 F32 = jnp.float32
+
+
+def watch_squares_in(frame):
+    piece_out = jnp.concatenate(
+        jax.lax.all_to_all(jnp.stack(jax.lax.axis_size(RA) * [frame], 0), RA, 0, 0), 0
+    )
+    return piece_out
 
 
 def turned(value, axis, steps):
@@ -96,7 +103,7 @@
         jnp.concatenate([w[l].astype(BF) for w in (up_weight, gate_weight, down_weight)], axis=1)
         for l in range(layers)
     ]
-    weights = [lax.all_gather(s, RA, axis=0, tiled=True) for s in shards]
+    weights = [watch_squares_in(s) for s in shards]
     own = lax.dynamic_slice_in_dim(tokens, cb * part, part, 0)
     own = own.reshape(part, ra, span).transpose(1, 0, 2)
     own = lax.all_to_all(own, RA, split_axis=0, concat_axis=0, tiled=True)

time: 321 us -> 678 us (2.11)
  waiting for transfers between devices: 126 us -> 367 us
  blocking collectives: 43.2 us -> 127 us
  starting transfers between devices: 52.2 us -> 80.5 us
  between operations: 14.3 us -> 0.9 us
  local copies, waits for them, and re-layouts: 39.1 us -> 50 us
  matrix products: 19.4 us -> 26.5 us
    all_to_all x0 -> x3, waiting for transfers between devices: none -> 294 us  [the longest x2 284 us: watch_squares_in(): jax.lax.all_to_all(jnp.stack(jax.lax.axis_size(RA) * [frame], 0), RA, 0, 0)]
    all_to_all x1, blocking collectives: 19.9 us -> 127 us  [per_device(): piece = lax.all_to_all(piece, RA, split_axis=0, concat_axis=0, tiled=True)]
    all_gather x2 -> x0, waiting for transfers between devices: 54.4 us -> none  [per_device(): weights = [lax.all_gather(s, RA, axis=0, tiled=True) for s in shards]]
    all_to_all x0 -> x3, starting transfers between devices: none -> 23.5 us  [the longest x1 12 us: per_device(): own = lax.all_to_all(own, RA, split_axis=0, concat_axis=0, tiled=True)]
    all_to_all x1 -> x0, blocking collectives: 23.3 us -> none  [per_device(): own = lax.all_to_all(own, RA, split_axis=0, concat_axis=0, tiled=True)]
    another operation x0 -> x2, local copies, waits for them, and re-layouts: none -> 9.39 us  [watch_squares_in(): jnp.stack(jax.lax.axis_size(RA) * [frame], 0)]
  transfers between devices with their start and end apart: 29 -> 30, of which waited for: 17 -> 19; matrix products, arithmetic and copies ran while one was open for 19% -> 9% of each run, Pallas kernels for 0% -> 0%
where the time goes in v1:
time: 678 us; the launch traced here: 671 us
  waiting for transfers between devices  367 us (54%)
  blocking collectives  127 us (19%)
  starting transfers between devices  80.5 us (12%)
  local copies, waits for them, and re-layouts  50 us (7%)
  matrix products  26.5 us (4%)
  other arithmetic  18.9 us (3%)
    all_to_all x2, waiting for transfers between devices, watch_squares_in(): jax.lax.all_to_all(jnp.stack(jax.lax.axis_size(RA) * [frame], 0), RA, 0, 0)  284 us
    all_to_all x1, blocking collectives, per_device(): piece = lax.all_to_all(piece, RA, split_axis=0, concat_axis=0, tiled=True)  127 us
    ppermute x25, waiting for transfers between devices, turned(): lax.ppermute(value, axis, [(s, (s + steps) % count) for s in range(count)])  73 us
    ppermute x25, starting transfers between devices, turned(): lax.ppermute(value, axis, [(s, (s + steps) % count) for s in range(count)])  50.9 us
  transfers between devices with their start and end apart: 30, of which 19 were waited for; matrix products, arithmetic and copies ran while one was open for 9% of the time, Pallas kernels for 0%

profile of v1, /device:TPU:1, one launch (start us, length us, event | category | flops | bytes accessed | tf_op | source)
XLA Modules:
  0.0 670.6 jit_solution(9980337736769563616)
XLA Ops:
  0.0 1.6 copy-done
  2.3 12.0 %all-to-all-start.1 = ((bf16[32,8,512]{2,1,0:T(8,128)(2,1)}), bf16[32,8,512]{2,1,0:T(8,128)(2,1)S(1)}, u32[]{:S(2)}, u32[]{:S(2)}) async-start(bf16[32,8,512]{2,1,0:T(8,128)(2,1)} %bitcast.5), calls=%async_computation.1 | async-start | bytes 524288 | tf_op jit(solution)/shard_map/all_to_all | solution.py:109
  16.5 9.1 %all-to-all-done.1 = bf16[32,8,512]{2,1,0:T(8,128)(2,1)S(1)} async-done(((bf16[32,8,512]{2,1,0:T(8,128)(2,1)}), bf16[32,8,512]{2,1,0:T(8,128)(2,1)S(1)}, u32[]{:S(2)}, u32[]{:S(2)}) %all-to-all-start.1) | async-done | bytes 262176 | tf_op jit(solution)/shard_map/all_to_all | solution.py:109
  25.7 4.7 stack.26
  30.3 5.0 all-to-all-start.2
  35.3 213.2 %all-to-all-done.2 = bf16[32,64,2304]{2,1,0:T(8,128)(2,1)} async-done(((bf16[32,64,2304]{2,1,0:T(8,128)(2,1)}), bf16[32,64,2304]{2,1,0:T(8,128)(2,1)}, u32[]{:S(2)}, u32[]{:S(2)}) %all-to-all-start.2) | async-done | bytes 9437216 | tf_op jit(solution)/shard_map/all_to_all | solution.py:17
  248.6 4.7 stack.22
  253.3 6.5 all-to-all-start
  261.1 1.5 collective-permute-start.1
  262.7 4.6 collective-permute-done
  267.4 2.7 collective-permute-start.3
  270.2 2.6 collective-permute-done.2
  272.8 3.4 collective-permute-start.4
  276.4 2.1 collective-permute-done.4
  279.3 1.7 copy.53
  281.2 3.2 collective-permute-start.5
  284.5 1.9 copy.54
  286.7 1.5 fusion.1
  288.3 5.1 multiply_multiply_fusion.3
  293.3 5.1 multiply_multiply_fusion.2
  298.4 4.6 fusion.20
  304.2 2.0 copy.68
  306.2 1.8 copy.69
  308.0 1.5 select_bitcast_fusion
  309.5 1.9 copy.58
  311.4 2.5 collective-permute-start.6
  314.0 2.4 collective-permute-done.6
  316.4 2.7 copy.59
  319.1 3.0 fusion.4
  323.4 2.4 collective-permute-start.9
  325.8 12.4 %collective-permute-done.7 = bf16[32,2048]{0,1:T(8,128)(2,1)S(1)} collective-permute-done((bf16[32,2048]{0,1:T(8,128)(2,1)S(1)}, bf16[32,2048]{0,1:T(8,128)(2,1)S(1)}, u32[]{:S(2)}, u32[]{:S(2)}) %collective-permute-start.7) | collective-permute-done | bytes 131104 | tf_op jit(solution)/shard_map/ppermute | solution.py:24
  340.0 2.0 collective-permute-start.10
  342.0 11.5 %collective-permute-done.8 = bf16[64,2048]{0,1:T(8,128)(2,1)S(1)} collective-permute-done((bf16[64,2048]{0,1:T(8,128)(2,1)S(1)}, bf16[64,2048]{0,1:T(8,128)(2,1)S(1)}, u32[]{:S(2)}, u32[]{:S(2)}) %collective-permute-start.8) | collective-permute-done | bytes 262176 | tf_op jit(solution)/shard_map/ppermute | solution.py:24
  353.5 1.7 fusion.55
  355.2 2.8 collective-permute-start.12
  358.4 9.7 %collective-permute-done.12 = bf16[64,2048]{0,1:T(8,128)(2,1)S(1)} collective-permute-done((bf16[64,2048]{0,1:T(8,128)(2,1)S(1)}, bf16[64,2048]{0,1:T(8,128)(2,1)S(1)}, u32[]{:S(2)}, u32[]{:S(2)}) %collective-permute-start.12) | collective-permute-done | bytes 262176 | tf_op jit(solution)/shard_map/ppermute | solution.py:24
  369.1 3.5 collective-permute-start.14
  375.0 7.3 %collective-permute-done.14 = bf16[32,2048]{0,1:T(8,128)(2,1)S(1)} collective-permute-done((bf16[32,2048]{0,1:T(8,128)(2,1)}, bf16[32,2048]{0,1:T(8,128)(2,1)S(1)}, u32[]{:S(2)}, u32[]{:S(2)}) %collective-permute-start.14) | collective-permute-done | bytes 131104 | tf_op jit(solution)/shard_map/ppermute | solution.py:24
  382.2 3.9 collective-permute-done.13
  386.7 3.1 collective-permute-start.15
  389.8 2.3 collective-permute-done.15
  392.5 3.0 collective-permute-start.16
  396.6 71.2 %all-to-all-done = bf16[32,64,2304]{2,1,0:T(8,128)(2,1)} async-done(((bf16[32,64,2304]{2,1,0:T(8,128)(2,1)}), bf16[32,64,2304]{2,1,0:T(8,128)(2,1)}, u32[]{:S(2)}, u32[]{:S(2)}) %all-to-all-start) | async-done | bytes 9437216 | tf_op jit(solution)/shard_map/all_to_all | solution.py:17
  467.9 3.8 multiply_multiply_fusion.1
  471.7 3.8 multiply_multiply_fusion
  475.5 4.2 fusion.17
  479.9 1.3 copy-done.2
  481.3 6.5 collective-permute-start.17
  487.8 2.4 collective-permute-done.17
  490.3 2.3 fusion.23
  492.6 1.3 collective-permute-start.18
  493.9 1.5 collective-permute-start.20
  495.4 3.2 collective-permute-done.18
  500.4 1.9 collective-permute-start.21
  502.5 7.5 %copy.66 = bf16[4,2,64,2048]{2,1,0,3:T(2,128)(2,1)} copy(bf16[4,2,64,2048]{3,2,1,0:T(8,128)(2,1)S(1)} %pad_maximum_fusion.3) | data formatting | bytes 4194304 | tf_op jit(solution)/shard_map/stack | solution.py:52
  509.9 9.3 %reshape_reshape.3 = bf16[512,32,8,8]{0,3,2,1:T(8,128)(2,1)S(1)} reshape(bf16[4,2,64,2048]{2,1,0,3:T(2,128)(2,1)} %copy.66) | data formatting | bytes 4194304 | tf_op jit(solution)/shard_map/reshape;reshape | solution.py:141
  520.5 126.8 %all_to_all.20 = bf16[32,8,512]{2,1,0:T(8,128)(2,1)S(1)} all-to-all(bf16[32,8,512]{2,1,0:T(8,128)(2,1)S(1)} %fusion.72), channel_id=1, replica_groups=mesh['z'=8,'y'=4,'x'=4,'c'=2] {'z','y'}, dimensions={0} | all-to-all | bytes 524288 | tf_op jit(solution)/shard_map/all_to_all | solution.py:147
  647.3 2.7 collective-permute-start.23
  650.1 3.6 collective-permute-done.22
  654.0 2.7 collective-permute-start.25
  656.8 2.6 collective-permute-done.24
  659.5 6.1 collective-permute-start.26
  665.7 2.3 collective-permute-done.26
  668.1 1.5 pad_maximum_fusion.4
  (112 shorter events, 20.8 us)
Async XLA Ops:
  0.0 1.6 copy-start
  0.0 16.4 %copy-start.7 = (f32[2,64,768]{2,1,0:T(8,128)S(1)}, f32[2,64,768]{2,1,0:T(8,128)}, u32[]{:S(2)}) copy-start(f32[2,64,768]{2,1,0:T(8,128)} %param.12) | copy-start | bytes 1179652
  2.3 23.3 %all-to-all-start.1 = ((bf16[32,8,512]{2,1,0:T(8,128)(2,1)}), bf16[32,8,512]{2,1,0:T(8,128)(2,1)S(1)}, u32[]{:S(2)}, u32[]{:S(2)}) async-start(bf16[32,8,512]{2,1,0:T(8,128)(2,1)} %bitcast.5), calls=%async_computation.1 | async-start | bytes 524288 | tf_op jit(solution)/shard_map/all_to_all | solution.py:109
  30.3 218.3 %all-to-all-start.2 = ((bf16[32,64,2304]{2,1,0:T(8,128)(2,1)}), bf16[32,64,2304]{2,1,0:T(8,128)(2,1)}, u32[]{:S(2)}, u32[]{:S(2)}) async-start(bf16[32,64,2304]{2,1,0:T(8,128)(2,1)} %stack.26), calls=%async_computation.2 | async-start | bytes 18874368 | tf_op jit(solution)/shard_map/all_to_all | solution.py:17
  253.3 214.6 %all-to-all-start = ((bf16[32,64,2304]{2,1,0:T(8,128)(2,1)}), bf16[32,64,2304]{2,1,0:T(8,128)(2,1)}, u32[]{:S(2)}, u32[]{:S(2)}) async-start(bf16[32,64,2304]{2,1,0:T(8,128)(2,1)} %stack.22), calls=%async_computation | async-start | bytes 18874368 | tf_op jit(solution)/shard_map/all_to_all | solution.py:17
  259.8 16.4 %copy-start.12 = (f32[2,768]{1,0:T(2,128)S(1)}, f32[2,768]{1,0:T(2,128)}, u32[]{:S(2)}) copy-start(f32[2,768]{1,0:T(2,128)} %param.15) | copy-start | bytes 18436
  259.8 16.5 %copy-start.8 = (f32[2,3,768]{2,0,1:T(2,128)S(1)}, f32[2,3,768]{2,0,1:T(2,128)}, u32[]{:S(2)}) copy-start(f32[2,3,768]{2,0,1:T(2,128)} %param.16) | copy-start | bytes 55300
  259.8 16.5 %copy-start.9 = (f32[2,3,768]{2,0,1:T(2,128)S(1)}, f32[2,3,768]{2,0,1:T(2,128)}, u32[]{:S(2)}) copy-start(f32[2,3,768]{2,0,1:T(2,128)} %param.17) | copy-start | bytes 55300
  259.8 16.6 %copy-start.10 = (f32[2,2048]{1,0:T(2,128)S(1)}, f32[2,2048]{1,0:T(2,128)}, u32[]{:S(2)}) copy-start(f32[2,2048]{1,0:T(2,128)} %param.11) | copy-start | bytes 49156
  259.8 7.4 %collective-permute-start = (bf16[32,8,512]{2,1,0:T(8,128)(2,1)S(1)}, bf16[32,8,512]{2,1,0:T(8,128)(2,1)S(1)}, u32[]{:S(2)}, u32[]{:S(2)}) collective-permute-start(bf16[32,8,512]{2,1,0:T(8,128)(2,1)S(1)} %all-to-all-done.1), channel_id=1, source_target_pairs={{0,2},{2,4},{4,6},{6,0},{1,3},{3,5},{5,7},{7,1},{8,10},{10,12},{12... | collective-permute-start | bytes 786440 | tf_op jit(solution)/shard_map/ppermute | solution.py:24
  261.1 6.2 collective-permute-start.1
  267.3 5.5 collective-permute-start.2
  267.4 5.4 collective-permute-start.3
  272.8 5.7 collective-permute-start.4
  278.8 5.6 copy-start.13
  279.1 5.4 copy-start.5
  281.2 5.2 collective-permute-start.5
  286.4 7.0 %copy-start.4 = (bf16[512,32,8,8]{0,3,2,1:T(8,128)(2,1)}, bf16[512,32,8,8]{0,3,2,1:T(8,128)(2,1)S(1)}, u32[]{:S(2)}) copy-start(bf16[512,32,8,8]{0,3,2,1:T(8,128)(2,1)S(1)} %copy.54) | copy-start | bytes 6291460
  311.4 5.0 collective-permute-start.6
  322.1 16.1 %copy-start.3 = (bf16[4,64,2048]{1,2,0:T(8,128)(2,1)}, bf16[4,64,2048]{1,2,0:T(8,128)(2,1)S(1)}, u32[]{:S(2)}) copy-start(bf16[4,64,2048]{1,2,0:T(8,128)(2,1)S(1)} %fusion.4) | copy-start | bytes 3145732
  322.6 15.6 %collective-permute-start.7 = (bf16[32,2048]{0,1:T(8,128)(2,1)S(1)}, bf16[32,2048]{0,1:T(8,128)(2,1)S(1)}, u32[]{:S(2)}, u32[]{:S(2)}) collective-permute-start(bf16[32,2048]{0,1:T(8,128)(2,1)S(1)} %get-tuple-element.27), channel_id=1, source_target_pairs={{0,2},{2,4},{4,6},{6,0},{1,3},{3,5},{5,7},{7,1},{8,10},{10,12},{12... | collective-permute-start | bytes 393224 | tf_op jit(solution)/shard_map/ppermute | solution.py:24
  323.4 14.8 %collective-permute-start.9 = (bf16[32,2048]{0,1:T(8,128)(2,1)S(1)}, bf16[32,2048]{0,1:T(8,128)(2,1)S(1)}, u32[]{:S(2)}, u32[]{:S(2)}) collective-permute-start(bf16[32,2048]{0,1:T(8,128)(2,1)S(1)} %get-tuple-element.29), channel_id=1, source_target_pairs={{0,6},{2,0},{4,2},{6,4},{1,7},{3,1},{5,3},{7,5},{8,14},{10,8},{12,... | collective-permute-start | bytes 393224 | tf_op jit(solution)/shard_map/ppermute | solution.py:24
  338.6 3.4 copy-start.11
  338.9 14.7 %collective-permute-start.8 = (bf16[64,2048]{0,1:T(8,128)(2,1)S(1)}, bf16[64,2048]{0,1:T(8,128)(2,1)S(1)}, u32[]{:S(2)}, u32[]{:S(2)}) collective-permute-start(bf16[64,2048]{0,1:T(8,128)(2,1)S(1)} %pad_maximum_fusion.7), channel_id=1, source_target_pairs={{0,2},{2,4},{4,6},{6,0},{1,3},{3,5},{5,7},{7,1},{8,10},{10,12},{12... | collective-permute-start | bytes 786440 | tf_op jit(solution)/shard_map/ppermute | solution.py:24
  340.0 13.6 %collective-permute-start.10 = (bf16[64,2048]{0,1:T(8,128)(2,1)S(1)}, bf16[64,2048]{0,1:T(8,128)(2,1)S(1)}, u32[]{:S(2)}, u32[]{:S(2)}) collective-permute-start(bf16[64,2048]{0,1:T(8,128)(2,1)S(1)} %pad_maximum_fusion.8), channel_id=1, source_target_pairs={{0,6},{2,0},{4,2},{6,4},{1,7},{3,1},{5,3},{7,5},{8,14},{10,8},{12,... | collective-permute-start | bytes 786440 | tf_op jit(solution)/shard_map/ppermute | solution.py:24
  355.2 12.9 %collective-permute-start.12 = (bf16[64,2048]{0,1:T(8,128)(2,1)S(1)}, bf16[64,2048]{0,1:T(8,128)(2,1)S(1)}, u32[]{:S(2)}, u32[]{:S(2)}) collective-permute-start(bf16[64,2048]{0,1:T(8,128)(2,1)S(1)} %fusion.55), channel_id=1, source_target_pairs={{0,6},{2,0},{4,2},{6,4},{1,7},{3,1},{5,3},{7,5},{8,14},{10,8},{12,... | collective-permute-start | bytes 786440 | tf_op jit(solution)/shard_map/ppermute | solution.py:24
  358.1 14.6 %collective-permute-start.11 = (bf16[64,2048]{0,1:T(8,128)(2,1)S(1)}, bf16[64,2048]{0,1:T(8,128)(2,1)S(1)}, u32[]{:S(2)}, u32[]{:S(2)}) collective-permute-start(bf16[64,2048]{0,1:T(8,128)(2,1)S(1)} %fusion.55), channel_id=1, source_target_pairs={{0,2},{2,4},{4,6},{6,0},{1,3},{3,5},{5,7},{7,1},{8,10},{10,12},{12... | collective-permute-start | bytes 786440 | tf_op jit(solution)/shard_map/ppermute | solution.py:24
  369.1 13.1 %collective-permute-start.14 = (bf16[32,2048]{0,1:T(8,128)(2,1)}, bf16[32,2048]{0,1:T(8,128)(2,1)S(1)}, u32[]{:S(2)}, u32[]{:S(2)}) collective-permute-start(bf16[32,2048]{0,1:T(8,128)(2,1)} %slice.372), channel_id=1, source_target_pairs={{0,6},{2,0},{4,2},{6,4},{1,7},{3,1},{5,3},{7,5},{8,14},{10,8},{12,... | collective-permute-start | bytes 393224 | tf_op jit(solution)/shard_map/ppermute | solution.py:24
  372.6 0.8 copy-start.6
  373.4 12.7 %collective-permute-start.13 = (bf16[32,2048]{0,1:T(8,128)(2,1)}, bf16[32,2048]{0,1:T(8,128)(2,1)S(1)}, u32[]{:S(2)}, u32[]{:S(2)}) collective-permute-start(bf16[32,2048]{0,1:T(8,128)(2,1)} %bitcast.158), channel_id=1, source_target_pairs={{0,2},{2,4},{4,6},{6,0},{1,3},{3,5},{5,7},{7,1},{8,10},{10,12},{12... | collective-permute-start | bytes 393224 | tf_op jit(solution)/shard_map/ppermute | solution.py:24
  386.7 5.4 collective-permute-start.15
  392.5 3.3 collective-permute-start.16
  479.9 1.3 copy-start.2
  481.3 8.9 %collective-permute-start.17 = (bf16[4,32,8,512]{3,2,1,0:T(8,128)(2,1)S(1)}, bf16[4,32,8,512]{3,2,1,0:T(8,128)(2,1)}, u32[]{:S(2)}, u32[]{:S(2)}) collective-permute-start(bf16[4,32,8,512]{3,2,1,0:T(8,128)(2,1)S(1)} %select_bitcast_fusion.3), channel_id=1, source_target_pairs={{0,1},{1,0},{2,3},{3,2},{4,5},{5,4},{6,7},{7,6},{8,9},{9,8},{10,11... | collective-permute-start | bytes 3145736 | tf_op jit(solution)/shard_map/ppermute | solution.py:24
  492.6 6.0 collective-permute-start.18
  493.9 4.7 collective-permute-start.20
  498.7 20.6 %collective-permute-start.19 = (bf16[32,8,512]{2,1,0:T(8,128)(2,1)S(1)}, bf16[32,8,512]{2,1,0:T(8,128)(2,1)}, u32[]{:S(2)}, u32[]{:S(2)}) collective-permute-start(bf16[32,8,512]{2,1,0:T(8,128)(2,1)S(1)} %pad_maximum_fusion.11), channel_id=1, source_target_pairs={{0,2},{2,4},{4,6},{6,0},{1,3},{3,5},{5,7},{7,1},{8,10},{10,12},{12... | collective-permute-start | bytes 786440 | tf_op jit(solution)/shard_map/ppermute | solution.py:24
  500.4 18.9 %collective-permute-start.21 = (bf16[32,8,512]{2,1,0:T(8,128)(2,1)}, bf16[32,8,512]{2,1,0:T(8,128)(2,1)}, u32[]{:S(2)}, u32[]{:S(2)}) collective-permute-start(bf16[32,8,512]{2,1,0:T(8,128)(2,1)} %pad_maximum_fusion.12), channel_id=1, source_target_pairs={{0,6},{2,0},{4,2},{6,4},{1,7},{3,1},{5,3},{7,5},{8,14},{10,8},{12,... | collective-permute-start | bytes 786440 | tf_op jit(solution)/shard_map/ppermute | solution.py:24
  647.3 6.4 collective-permute-start.22
  647.3 6.6 collective-permute-start.23
  653.8 5.6 collective-permute-start.24
  654.0 5.4 collective-permute-start.25
  659.5 8.4 %collective-permute-start.26 = (bf16[4,8,16384]{2,1,0:T(8,128)(2,1)S(1)}, bf16[4,8,16384]{2,1,0:T(8,128)(2,1)S(1)}, u32[]{:S(2)}, u32[]{:S(2)}) collective-permute-start(bf16[4,8,16384]{2,1,0:T(8,128)(2,1)S(1)} %fusion.76), channel_id=1, source_target_pairs={{0,1},{1,0},{2,3},{3,2},{4,5},{5,4},{6,7},{7,6},{8,9},{9,8},{10,11... | collective-permute-start | bytes 3145736 | tf_op jit(solution)/shard_map/ppermute | solution.py:24
  668.1 2.4 copy-start.1
